TPU v7x, 32 devices: a whole 2x2x4 slice. The times are simulated.
32 devices in a mesh: grp: 2 (over y), sp: 4 (over z), tp: 4 (over x, core).
Axes of the slice: x: 2, y: 2, z: 4, core: 2. Of those that a mesh axis runs over, the one named last changes fastest.
Arguments:
- tokens: bfloat16 [2048, 2048], P(('grp', 'sp', 'tp')), parts along dimension 0, may hold values from -6 to 6
- norm_gain: float32 [2048], replicated, may hold values from 0.1 to 1.9
- conv_b_w: bfloat16 [2048, 1024], P('sp', 'tp'), may hold values from -0.125 to 0.125
- conv_c_w: bfloat16 [2048, 1024], P('sp', 'tp'), may hold values from -0.125 to 0.125
- conv_x_w: bfloat16 [2048, 1024], P('sp', 'tp'), may hold values from -0.125 to 0.125
- query_w: bfloat16 [2048, 1024], P('sp', 'tp'), may hold values from -1 to 1
- key_w: bfloat16 [2048, 256], P('sp', 'tp'), may hold values from -2 to 2
- value_w: bfloat16 [2048, 256], P('sp', 'tp'), may hold values from -0.125 to 0.125
- conv_taps: float32 [3, 1024], P(None, 'tp'), may hold values from -3.5 to 3.5
- gate_cache: float32 [2048, 16], P('grp', 'tp'), parts along dimension 0, as said below
- out_conv_w: bfloat16 [1024, 2048], P('tp'), may hold values from -0.1875 to 0.1875
- out_attn_w: bfloat16 [1024, 2048], P('tp'), may hold values from -0.75 to 0.75
Outputs:
- mixed: bfloat16 [2048, 2048], P(('grp', 'sp', 'tp')), parts along dimension 0
- log_total: float32 [2048, 16], P(('grp', 'sp'), 'tp'), parts along dimension 0
There are 2 independent parts, one for each index of `grp`. A program takes and returns all parts, laid end to end along the dimension named above; an argument that names none is the same for every part. Nothing has to cross between parts.
Inputs may be any that keep to these rules, and one draw needn't show every extreme that they name: `gate_cache`: never rises along positions; starts at or below zero.
All inputs are finite; a program needn't handle non-finite values.
Results may differ from a plain program's by a relative error of at most 0.017.
The roundings to bfloat16 on the way count: a program that leaves them out, or rounds other values in their place, can miss the bound.
Values may be sent and summed in bfloat16 or wider, within the bound.
A program may use at most 64 MiB of HBM per device.

v0:
```python
import functools

import jax
import jax.numpy as jnp
from jax import lax
from jax.experimental import pallas as pl
from jax.experimental.pallas import tpu as pltpu
from jax.sharding import PartitionSpec as P

HD = 64
LANES = 128
MESH = pl.DeviceIdType.MESH
F32 = jnp.float32
BF16 = jnp.bfloat16


def layer_kernel(
    n_sp,
    n_tp,
    tokens_ref,
    gain_ref,
    wb_hbm,
    wc_hbm,
    wx_hbm,
    wq_hbm,
    wk_hbm,
    wv_hbm,
    taps_ref,
    gate_ref,
    oconv_ref,
    oattn_ref,
    mixed_ref,
    lse_ref,
    tok,
    normed,
    packed,
    wmain,
    wkv,
    proj,
    outs,
    comb,
    lse_out,
    lse_in,
    wout,
    part,
    sib,
    fwd,
    xin,
    wb_ref,
    wc_ref,
    wx_ref,
    wq_ref,
    wk_ref,
    wv_ref,
    send_sem,
    tok_sem,
    main_sem,
    kv_sem,
    out_sem,
    sum_sem,
    local_sem,
):
    g = lax.axis_index("grp")
    s = lax.axis_index("sp")
    t = lax.axis_index("tp")
    across = {"grp": 1 - g}
    sibling = t + 1 - 2 * lax.rem(t, 2)
    far = lax.rem(t + 2, n_tp)
    far_sibling = lax.rem(sibling + 2, n_tp)
    depth = wb_hbm.shape[0]
    half = depth // 2
    rows_own, width = tokens_ref.shape
    count = rows_own * n_tp
    total = count * n_sp
    sub = rows_own // 2
    ch = wb_hbm.shape[1] // n_sp

    def block(index, size):
        return pl.ds(pl.multiple_of(index * size, size), size)

    local = []
    for d in range(n_sp):
        for k, ref in ((0, oconv_ref), (1, oattn_ref)):
            local.append(
                pltpu.make_async_copy(
                    ref.at[pl.ds(d * ch, ch)],
                    wout.at[pl.ds((2 * d + k) * ch, ch)],
                    local_sem.at[2 * d + k],
                )
            )
    weights_in = [
        pltpu.make_async_copy(src, dst, local_sem.at[2 * n_sp + k])
        for k, (src, dst) in enumerate(
            (
                (wb_hbm, wb_ref),
                (wc_hbm, wc_ref),
                (wx_hbm, wx_ref),
                (wq_hbm, wq_ref),
                (wk_hbm, wk_ref),
                (wv_hbm, wv_ref),
            )
        )
    ]
    for copy in weights_in + local:
        copy.start()

    barrier = pltpu.get_barrier_semaphore()
    for by in range(1, n_sp):
        pl.semaphore_signal(
            barrier, inc=1, device_id={"sp": lax.rem(s + by, n_sp)}, device_id_type=MESH
        )
    for by in range(1, n_tp):
        pl.semaphore_signal(
            barrier, inc=1, device_id={"tp": lax.rem(t + by, n_tp)}, device_id_type=MESH
        )
    pl.semaphore_signal(barrier, inc=1, device_id=across, device_id_type=MESH)
    pl.semaphore_wait(barrier, n_sp + n_tp - 1)

    used = [0]
    sent = []

    def send(src, dst, arrival, device, when=None):
        index = used[0]
        used[0] += 1
        copy = pltpu.make_async_remote_copy(
            src_ref=src,
            dst_ref=dst,
            send_sem=send_sem.at[index],
            recv_sem=arrival,
            device_id=device,
            device_id_type=MESH,
        )
        sent.append((copy, when))
        if when is None:
            copy.start()
        else:
            pl.when(when)(copy.start)
        return copy

    def arrived(ref, arrival):
        pltpu.make_async_remote_copy(
            src_ref=ref,
            dst_ref=ref,
            send_sem=send_sem.at[0],
            recv_sem=arrival,
            device_id=across,
            device_id_type=MESH,
        ).wait_recv()

    def both(a, b):
        return b if a is None else jnp.logical_and(a, b)

    def tok_block(z, x, p):
        return tok.at[block((z * n_tp + x) * 2 + p, sub)]

    def tok_arrival(z, x, p):
        return tok_sem.at[(z * n_tp + x) * 2 + p]

    def tok_spread(src, z, p, step, when):
        arrival = tok_arrival(z, t, p)
        dst = tok_block(z, t, p)
        if step >= 0:
            send(src, dst, arrival, {"sp": lax.rem(s + 1, n_sp)}, both(when, s < n_sp - 1))
        if step <= 0:
            send(src, dst, arrival, {"sp": lax.rem(s + n_sp - 1, n_sp)}, both(when, s > 0))
        send(src, dst, arrival, {"tp": far}, when)
        send(src, dst, arrival, {"tp": sibling}, when)

    def tok_round(h):
        for p in range(2):
            for step in (1, -1):
                z = lax.rem(s - step * h + n_sp, n_sp)
                exists = (s >= h) if step > 0 else (s + h < n_sp)

                @pl.when(exists)
                def _(z=z):
                    arrived(tok_block(z, t, p), tok_arrival(z, t, p))

                tok_spread(tok_block(z, t, p), z, p, step, exists)

    def tok_far(z, when=None):
        for p in range(2):
            arrival = tok_arrival(z, far, p)
            here = tok_block(z, far, p)

            @pl.when(True if when is None else when)
            def _():
                arrived(here, arrival)

            send(here, here, arrival, {"tp": sibling}, when)

    def far_round(h):
        for step in (1, -1):
            exists = (s >= h) if step > 0 else (s + h < n_sp)
            tok_far(lax.rem(s - step * h + n_sp, n_sp), exists)

    def main_rows(z, g_half):
        return wmain.at[block(2 * z + g_half, half)]

    def kv_rows(z, g_half):
        return wkv.at[block(2 * z + g_half, half)]

    def weights_out(h):
        for step in (1, -1):
            exists = (s + h < n_sp) if step > 0 else (s >= h)
            d = lax.rem(s + step * h + n_sp, n_sp)
            to = {"sp": d}
            send(kv_rows(s, g), kv_rows(s, g), kv_sem.at[s], to, exists)
            send(packed.at[d, block(g, half)], main_rows(s, g), main_sem.at[s], to, exists)

    def weights_over(h):
        for step in (1, -1):
            exists = (s >= h) if step > 0 else (s + h < n_sp)
            z = lax.rem(s - step * h + n_sp, n_sp)
            for rows, sems in ((kv_rows, kv_sem), (main_rows, main_sem)):

                @pl.when(exists)
                def _(rows=rows, sems=sems, z=z):
                    arrived(rows(z, g), sems.at[z])

                send(rows(z, g), rows(z, g), sems.at[n_sp + z], across, exists)

    for p in range(2):
        tok_spread(tokens_ref.at[pl.ds(p * sub, sub)], s, p, 0, None)
    tok[block(s * n_tp + t, rows_own), :] = tokens_ref[...]
    for copy in weights_in:
        copy.wait()
    for d in range(n_sp):
        cols = slice(d * ch, (d + 1) * ch)
        packed[d, :, : 2 * ch] = jnp.concatenate([wb_ref[:, cols], wc_ref[:, cols]], axis=1)
        packed[d, :, 2 * ch :] = jnp.concatenate([wx_ref[:, cols], wq_ref[:, cols]], axis=1)
    stacked = jnp.concatenate([wk_ref[...], wv_ref[...]], axis=0).astype(F32)
    wkv[block(s, depth), :] = stacked.T.astype(BF16)
    wmain[block(s, depth), :] = packed[s]

    tok_round(1)
    for h in range(1, n_sp):
        weights_out(h)
    tok_far(s)
    for h in range(2, n_sp):
        tok_round(h)
        far_round(h - 1)
        weights_over(h - 1)
    weights_over(n_sp - 1)
    far_round(n_sp - 1)
    for by in range(n_sp):
        z = lax.rem(s + by, n_sp)
        for p in range(2):
            for x in (sibling, far_sibling):
                arrived(tok_block(z, x, p), tok_arrival(z, x, p))

    def normalize(i, unused):
        rows = block(i, rows_own)
        xf = tok[rows, :].astype(F32)
        square = jnp.sum(xf * xf, axis=-1, keepdims=True)
        normed[rows, :] = (xf * gain_ref[...]).astype(BF16)
        scale = lax.rsqrt(square / width + 1e-05)
        proj[rows, :] = jnp.broadcast_to(scale, (rows_own, proj.shape[1]))
        return unused

    lax.fori_loop(0, n_sp * n_tp, normalize, 0)
    scale_rows = proj[:, :1]
    gate_row = gate_ref[pl.ds(s, 1), :]
    gate_column = jnp.broadcast_to(gate_row, (LANES, total)).T[:, :1]
    taps = taps_ref.shape[0]
    taps_own = jnp.zeros((taps, ch), F32)
    for d in range(n_sp):
        taps_own = jnp.where(s == d, taps_ref[:, d * ch : (d + 1) * ch], taps_own)

    for by in range(1, n_sp):
        z = lax.rem(s + by, n_sp)
        arrived(main_rows(z, 1 - g), main_sem.at[n_sp + z])
        arrived(kv_rows(z, 1 - g), kv_sem.at[n_sp + z])

    def project(weight):
        return (
            jnp.dot(normed[...], weight, preferred_element_type=F32) * scale_rows
        ).astype(BF16)

    main = project(wmain[...])
    kv = project(wkv[...])
    gate_b = main[:, :ch].astype(F32)
    conv_src = main[:, ch : 2 * ch].astype(F32) * main[:, 2 * ch : 3 * ch].astype(F32)
    conv_src = conv_src.astype(BF16).astype(F32)
    filtered = jnp.zeros((total, ch), F32)
    for tap in range(taps):
        back = taps - 1 - tap
        moved = conv_src
        if back:
            moved = jnp.concatenate([jnp.zeros((back, ch), F32), conv_src[: total - back]], axis=0)
        filtered = filtered + taps_own[tap : tap + 1] * moved
    conv_out = (gate_b * filtered).astype(BF16)
    query = main[:, 3 * ch :] * BF16(HD**-0.5)
    keys, values = kv[:, :HD], kv[:, HD:]
    for d in reversed(range(n_sp)):
        rows = slice(d * count, (d + 1) * count)
        seen = (d + 1) * count
        score = lax.dot_general(
            query[rows],
            keys[:seen],
            (((1,), (1,)), ((), ())),
            preferred_element_type=F32,
        )
        score = score + gate_column[rows] - gate_row[:, :seen]
        q_pos = d * count + lax.broadcasted_iota(jnp.int32, (count, seen), 0)
        visible = lax.broadcasted_iota(jnp.int32, (count, seen), 1) <= q_pos
        score = jnp.where(visible, score, -1e30)
        row_max = jnp.max(score, axis=-1, keepdims=True)
        weight = jnp.exp(score - row_max)
        row_sum = jnp.sum(weight, axis=-1, keepdims=True)
        out = jnp.dot(weight.astype(BF16), values[:seen], preferred_element_type=F32)
        attn_out = (out / row_sum).astype(BF16)
        both_out = jnp.concatenate([conv_out[rows], attn_out], axis=1)
        for r in range(2):
            for k in range(n_tp):
                start = k * rows_own + r * sub
                outs[r, d, k * sub : (k + 1) * sub] = both_out[start : start + sub]
        logs = jnp.broadcast_to(row_max + jnp.log(row_sum), (count, LANES)).T
        lse_out[d] = logs[: lse_out.shape[1]]
        other = s != d
        send(outs.at[0, d], comb.at[0, s], out_sem.at[s], {"sp": d}, other)
    for d in range(n_sp):
        other = s != d
        send(outs.at[1, d], comb.at[1, s], out_sem.at[n_sp + s], {"sp": d}, other)
        send(lse_out.at[d], lse_in.at[s], out_sem.at[2 * n_sp + s], {"sp": d}, other)
    for r in range(2):
        comb[r, s] = outs[r, s]
    lse_in[s] = lse_out[s]
    for copy in local:
        copy.wait()

    chunks = 2
    wide = width // chunks

    def relay(r, c):
        cols = pl.ds(c * wide, wide)
        base = 3 * (chunks * r + c)
        for k in range(2):
            arrived(sib.at[r, k, :, cols], sum_sem.at[base + k])
        pair = part[r, far, :, cols].astype(F32) + sib[r, 1, :, cols].astype(F32)
        fwd[r, :, cols] = pair.astype(BF16)
        send(fwd.at[r, :, cols], xin.at[r, :, cols], sum_sem.at[base + 2], {"tp": far})

    last = None
    for r in range(2):
        for by in range(1, n_sp):
            z = lax.rem(s + by, n_sp)
            arrived(comb.at[r, z], out_sem.at[r * n_sp + z])
        gathered = jnp.concatenate([comb[r, d] for d in range(n_sp)], axis=1)
        for c in range(chunks):
            cols = pl.ds(c * wide, wide)
            term = jnp.dot(gathered, wout[:, cols], preferred_element_type=F32).astype(BF16)
            for k in range(n_tp):
                part[r, k, :, cols] = term[k * sub : (k + 1) * sub]
            for k, owner in ((1, far_sibling), (0, sibling)):
                send(
                    part.at[r, owner, :, cols],
                    sib.at[r, k, :, cols],
                    sum_sem.at[3 * (chunks * r + c) + k],
                    {"tp": sibling},
                )
            if last is not None:
                relay(*last)
            last = (r, c)
    relay(*last)
    for by in range(1, n_sp):
        z = lax.rem(s + by, n_sp)
        arrived(lse_in.at[z], out_sem.at[2 * n_sp + z])
    for d in range(n_sp):
        lse_ref[d : d + 1, :] = lse_in[d, :1]
    for r in range(2):
        for c in range(chunks):
            cols = pl.ds(c * wide, wide)
            arrived(xin.at[r, :, cols], sum_sem.at[3 * (chunks * r + c) + 2])
            whole = part[r, t, :, cols].astype(F32) + sib[r, 0, :, cols].astype(F32)
            whole = whole + xin[r, :, cols].astype(F32)
            mixed_ref[r * sub : (r + 1) * sub, cols] = whole.astype(BF16)
    for copy, when in sent:
        if when is None:
            copy.wait_send()
        else:
            pl.when(when)(copy.wait_send)


COPIES = 192


def in_one_kernel(
    n_sp,
    n_tp,
    tokens,
    norm_gain,
    conv_b_w,
    conv_c_w,
    conv_x_w,
    query_w,
    key_w,
    value_w,
    conv_taps,
    gate_cache,
    out_conv_w,
    out_attn_w,
):
    rows, width = tokens.shape
    count = rows * n_tp
    depth, channels = conv_b_w.shape
    heads = gate_cache.shape[1]
    kv_width = key_w.shape[1] + value_w.shape[1]
    total = gate_cache.shape[0]
    main_width = (3 * channels + query_w.shape[1]) // n_sp
    pair_width = (channels + query_w.shape[1]) // n_sp
    vmem = pl.BlockSpec(memory_space=pltpu.VMEM)
    hbm = pl.BlockSpec(memory_space=pl.ANY)
    out_rows = out_conv_w.shape[0] + out_attn_w.shape[0]
    dma = pltpu.SemaphoreType.DMA
    mixed, log_rows = pl.pallas_call(
        functools.partial(layer_kernel, n_sp, n_tp),
        out_shape=(
            jax.ShapeDtypeStruct((rows, width), BF16),
            jax.ShapeDtypeStruct((heads, count), F32),
        ),
        in_specs=[vmem] * 2 + [hbm] * 6 + [vmem] * 2 + [hbm] * 2,
        out_specs=(vmem, vmem),
        scratch_shapes=[
            pltpu.VMEM((total, width), BF16),
            pltpu.VMEM((total, width), BF16),
            pltpu.VMEM((n_sp, depth, main_width), BF16),
            pltpu.VMEM((width, main_width), BF16),
            pltpu.VMEM((width, kv_width), BF16),
            pltpu.VMEM((total, LANES), F32),
            pltpu.VMEM((2, n_sp, count // 2, pair_width), BF16),
            pltpu.VMEM((2, n_sp, count // 2, pair_width), BF16),
            pltpu.VMEM((n_sp, 8, count), F32),
            pltpu.VMEM((n_sp, 8, count), F32),
            pltpu.VMEM((out_rows, width), BF16),
            pltpu.VMEM((2, n_tp, rows // 2, width), BF16),
            pltpu.VMEM((2, 2, rows // 2, width), BF16),
            pltpu.VMEM((2, rows // 2, width), BF16),
            pltpu.VMEM((2, rows // 2, width), BF16),
            pltpu.VMEM(conv_b_w.shape, BF16),
            pltpu.VMEM(conv_c_w.shape, BF16),
            pltpu.VMEM(conv_x_w.shape, BF16),
            pltpu.VMEM(query_w.shape, BF16),
            pltpu.VMEM(key_w.shape[::-1], BF16),
            pltpu.VMEM(value_w.shape[::-1], BF16),
            dma((COPIES,)),
            dma((2 * n_sp * n_tp,)),
            dma((2 * n_sp,)),
            dma((2 * n_sp,)),
            dma((3 * n_sp,)),
            dma((12,)),
            dma((2 * n_sp + 6,)),
        ],
        compiler_params=pltpu.CompilerParams(
            collective_id=0, has_side_effects=True, vmem_limit_bytes=60 * 1024 * 1024
        ),
    )(
        tokens,
        norm_gain.reshape(1, width),
        conv_b_w,
        conv_c_w,
        conv_x_w,
        query_w,
        key_w.T,
        value_w.T,
        conv_taps,
        gate_cache.T,
        out_conv_w,
        out_attn_w,
    )
    return mixed, log_rows.T


def passed_along(value, axis, by):
    count = lax.axis_size(axis)
    pairs = [(i, i + by) for i in range(count) if 0 <= i + by < count]
    return lax.ppermute(value, axis, pairs)


def on_device(
    tokens,
    norm_gain,
    conv_b_w,
    conv_c_w,
    conv_x_w,
    query_w,
    key_w,
    value_w,
    conv_taps,
    gate_cache,
    out_conv_w,
    out_attn_w,
):
    rows = lax.all_gather(tokens, "tp", axis=0, tiled=True)
    count = rows.shape[0]
    xf = rows.astype(jnp.float32)
    scale_rows = lax.rsqrt(jnp.mean(xf * xf, axis=-1, keepdims=True) + 1e-05)
    normed = (xf * norm_gain).astype(jnp.bfloat16)

    def contract_all(pieces):
        width = pieces[0].shape[0]
        return tuple(
            (jnp.dot(normed, piece, preferred_element_type=jnp.float32) for piece in pieces)
        )

    conv_sums = contract_all(
        (
            lax.all_gather(conv_b_w, "sp", axis=0, tiled=True),
            lax.all_gather(conv_c_w, "sp", axis=0, tiled=True),
            lax.all_gather(conv_x_w, "sp", axis=0, tiled=True),
        )
    )
    attn_sums = contract_all(
        (
            lax.all_gather(query_w, "sp", axis=0, tiled=True),
            lax.all_gather(key_w, "sp", axis=0, tiled=True),
            lax.all_gather(value_w, "sp", axis=0, tiled=True),
        )
    )
    sums = conv_sums + attn_sums
    gate_b, gate_c, conv_in, query, key, value = [
        (total * scale_rows).astype(jnp.bfloat16) for total in sums
    ]
    taps = conv_taps.shape[0]
    channels = conv_in.shape[1]
    conv_src = (gate_c.astype(jnp.float32) * conv_in.astype(jnp.float32)).astype(jnp.bfloat16)
    earlier = passed_along(conv_src[count - (taps - 1) :], "sp", 1)
    padded = jnp.concatenate([earlier, conv_src], axis=0)
    filtered = jnp.zeros((count, channels), jnp.float32)
    for tap in range(taps):
        filtered = filtered + conv_taps[tap][None, :] * padded[tap : tap + count].astype(
            jnp.float32
        )
    conv_out = (gate_b.astype(jnp.float32) * filtered).astype(jnp.bfloat16)
    heads_dev = gate_cache.shape[1]
    kv_dev = key.shape[1] // HD
    group = heads_dev // kv_dev
    half = count // 2
    sp_index = lax.axis_index("sp")
    own_start = sp_index * count
    scale = HD ** (-0.5)
    later_query = query[half:]
    later_start = own_start + half

    def prepare(q_rows, begin):
        heads_q = q_rows.reshape(half, kv_dev, group, HD)
        q_gate = lax.dynamic_slice_in_dim(gate_cache, begin, half, 0).T.reshape(
            kv_dev, group, half, 1
        )
        q_pos = begin + jnp.arange(half, dtype=jnp.int32)
        return (heads_q, q_gate, q_pos)

    sides = (prepare(query[:half], own_start), prepare(later_query, later_start))

    def absorb(carry, side, key_rows, value_rows, begin):
        heads_q, q_gate, q_pos = side
        run_max, run_sum, acc = carry
        width = key_rows.shape[0]
        key_heads = key_rows.reshape(width, kv_dev, HD)
        value_heads = value_rows.reshape(width, kv_dev, HD)
        score = (
            jnp.einsum("qgjd,kgd->gjqk", heads_q, key_heads, preferred_element_type=jnp.float32)
            * scale
        )
        key_gate = lax.dynamic_slice_in_dim(gate_cache, begin, width, 0).T.reshape(
            kv_dev, group, 1, width
        )
        score = score + q_gate - key_gate
        mask = (begin + jnp.arange(width, dtype=jnp.int32))[None, :] <= q_pos[:, None]
        score = jnp.where(mask, score, -1e30)
        new_max = jnp.maximum(run_max, jnp.max(score, axis=-1))
        weight = jnp.where(mask, jnp.exp(score - new_max[..., None]), 0.0)
        factor = jnp.exp(run_max - new_max)
        new_sum = run_sum * factor + jnp.sum(weight, axis=-1)
        product = jnp.einsum(
            "gjqk,kgd->gjqd",
            weight.astype(jnp.bfloat16),
            value_heads,
            preferred_element_type=jnp.float32,
        )
        return (new_max, new_sum, acc * factor[..., None] + product)

    def guarded(carry, side, key_rows, value_rows, begin):

        def visit_rows(state):
            return absorb(state, side, key_rows, value_rows, begin)

        def keep(state):
            return state

        return lax.cond(begin <= side[2][half - 1], visit_rows, keep, carry)

    def absorb_both(carry, key_rows, value_rows, begin):
        return (
            guarded(carry[0], sides[0], key_rows, value_rows, begin),
            guarded(carry[1], sides[1], key_rows, value_rows, begin),
        )

    def fresh():
        return (
            jnp.full((kv_dev, group, half), -1e30, jnp.float32),
            jnp.zeros((kv_dev, group, half), jnp.float32),
            jnp.zeros((kv_dev, group, half, HD), jnp.float32),
        )

    key_rows = lax.all_gather(key, "sp", axis=0, tiled=True)
    value_rows = lax.all_gather(value, "sp", axis=0, tiled=True)
    width = key_rows.shape[0]
    step = 512
    key_blocks = key_rows.reshape(width // step, step, key_rows.shape[1])
    value_blocks = value_rows.reshape(width // step, step, value_rows.shape[1])
    firsts = step * jnp.arange(width // step, dtype=jnp.int32)

    def visit(state, inputs):
        return (absorb_both(state, inputs[0], inputs[1], inputs[2]), None)

    result, unused = lax.scan(visit, (fresh(), fresh()), (key_blocks, value_blocks, firsts))

    def finish(state):
        run_max, run_sum, acc = state
        out = (
            (acc / run_sum[..., None])
            .transpose(2, 0, 1, 3)
            .reshape(half, heads_dev * HD)
            .astype(jnp.bfloat16)
        )
        lse = (run_max + jnp.log(run_sum)).transpose(2, 0, 1).reshape(half, heads_dev)
        return (out, lse)

    early_out, early_lse = finish(result[0])
    later_out, later_lse = finish(result[1])
    attn_out = jnp.concatenate([early_out, later_out], axis=0)
    log_total = jnp.concatenate([early_lse, later_lse], axis=0)
    term = jnp.dot(conv_out, out_conv_w, preferred_element_type=jnp.float32)
    mixed = lax.psum_scatter(
        (term + jnp.dot(attn_out, out_attn_w, preferred_element_type=jnp.float32)).astype(
            jnp.bfloat16
        ),
        "tp",
        scatter_dimension=0,
        tiled=True,
    )
    return (mixed, log_total)


def solution(mesh):
    placed = (
        P(("grp", "sp", "tp"), None),
        P(),
        P("sp", "tp"),
        P("sp", "tp"),
        P("sp", "tp"),
        P("sp", "tp"),
        P("sp", "tp"),
        P("sp", "tp"),
        P(None, "tp"),
        P("grp", "tp"),
        P("tp", None),
        P("tp", None),
    )
    sizes = dict(mesh.shape)

    def on_one(*args):
        channels, key_width = args[2].shape[1], args[6].shape[1]
        grid = (sizes["grp"], sizes["sp"], sizes["tp"])
        fits = channels == sizes["sp"] * HD and key_width == HD
        if grid == (2, 4, 4) and fits and args[9].shape[1] == sizes["sp"]:
            return in_one_kernel(sizes["sp"], sizes["tp"], *args)
        return on_device(*args)

    return jax.shard_map(
        on_one,
        mesh=mesh,
        in_specs=placed,
        out_specs=(P(("grp", "sp", "tp"), None), P(("grp", "sp"), "tp")),
        check_vma=False,
    )
```

profile of v0, /device:TPU:0, one launch (start us, length us, event | category | flops | bytes accessed | tf_op | source)
XLA Modules:
  0.0 69.6 jit_solution(2735218189843818345)
XLA Ops:
  0.6 66.7 %shard_map.131 = (bf16[64,2048]{1,0:T(8,128)(2,1)}, f32[4,256]{1,0:T(4,128)}) custom-call(bf16[64,2048]{1,0:T(8,128)(2,1)} %tokens_ref.1, f32[1,2048]{1,0:T(1,128)} %bitcast.8, bf16[512,256]{1,0:T(8,128)(2,1)} %wb_hbm.1, bf16[512,256]{1,0:T(8,128)(2,1)} %wc_hbm.1, bf16[512,256]{1,0:T(8,128)(2,1)} %wx_hbm.1, bf16[512,256]{1,0:T(8,128)(2,1)} %wq_hbm.1, ...), custom_call_target="tpu_custom_call" | custom-call | tf_op jit(solution)/shard_map/pallas_call | solution.py:416
  67.3 0.0 copy-start
  67.3 1.7 %copy.16 = bf16[64,2048]{1,0:T(8,128)(2,1)} copy(bf16[64,2048]{1,0:T(8,128)(2,1)} %get-tuple-element.8) | data formatting | bytes 524288
  69.0 0.0 copy-done
  69.0 0.6 copy.17
Async XLA Ops:
  67.3 1.7 %copy-start = (f32[4,256]{1,0:T(4,128)S(1)}, f32[4,256]{1,0:T(4,128)}, u32[]{:S(2)}) copy-start(f32[4,256]{1,0:T(4,128)} %get-tuple-element.5) | copy-start | bytes 12292
where the time goes:
time: 69.8 us; the launch traced here: 69.6 us
  Pallas kernels  66.7 us (96%)
  local copies, waits for them, and re-layouts  2.27 us (3%)
    pallas_call x1, Pallas kernels, in_one_kernel(): pl.pallas_call(functools.partial(layer_kernel, n_sp, n_tp), out_shape=(ja...  66.7 us
    unnamed x4, local copies, waits for them, and re-layouts  2.27 us

commit v1 on v0

v1 whole, which is shorter than its diff:
```python
import functools

import jax
import jax.numpy as jnp
from jax import lax
from jax.experimental import pallas as pl
from jax.experimental.pallas import tpu as pltpu
from jax.sharding import PartitionSpec as P

HD = 64
LANES = 128
MESH = pl.DeviceIdType.MESH
F32 = jnp.float32
BF16 = jnp.bfloat16


def layer_kernel(
    n_sp,
    n_tp,
    tokens_hbm,
    gain_hbm,
    wb_hbm,
    wc_hbm,
    wx_hbm,
    wq_hbm,
    wk_hbm,
    wv_hbm,
    taps_hbm,
    gate_hbm,
    oconv_hbm,
    oattn_hbm,
    mixed_ref,
    lse_ref,
    tok,
    normed,
    scale,
    gain,
    taps_own,
    taps_sib,
    gate_own,
    gate_sib,
    wb_ref,
    wc_ref,
    wx_ref,
    wq_ref,
    kv_ref,
    bc_all,
    x_all,
    q_all,
    kv_all,
    gates,
    pack,
    attn_o,
    conv_o,
    comb,
    lse_out,
    lse_in,
    wout,
    part,
    sib,
    fwd,
    xin,
    send_sem,
    tok_sem,
    w_sem,
    small_sem,
    kv_sem,
    out_sem,
    sum_sem,
    local_sem,
):
    g = lax.axis_index("grp")
    s = lax.axis_index("sp")
    t = lax.axis_index("tp")
    core = lax.rem(t, 2)
    first = t - core
    parity = lax.rem(s, 2)
    owner = core == parity
    across = {"grp": 1 - g}
    sibling = first + 1 - core
    far = lax.rem(t + 2, n_tp)
    far_sibling = lax.rem(sibling + 2, n_tp)
    z_near = s + 1 - 2 * parity
    z_two = lax.rem(s + 2, n_sp)
    z_three = n_sp - 1 - s
    late = s >= 2
    rows_own, width = tokens_hbm.shape
    depth = wb_hbm.shape[0]
    half = depth // 2
    count = rows_own * n_tp
    mine = 2 * count
    sub = rows_own // 2
    ch = wb_hbm.shape[1] // 2

    def block(index, size):
        return pl.ds(pl.multiple_of(index * size, size), size)

    barrier = pltpu.get_barrier_semaphore()
    for by in range(1, n_sp):
        for to in (t, sibling):
            pl.semaphore_signal(
                barrier,
                inc=1,
                device_id={"sp": lax.rem(s + by, n_sp), "tp": to},
                device_id_type=MESH,
            )
    for to in (sibling, far):
        pl.semaphore_signal(barrier, inc=1, device_id={"tp": to}, device_id_type=MESH)
    pl.semaphore_signal(barrier, inc=1, device_id=across, device_id_type=MESH)

    def tok_rows(z, x):
        return pl.ds(pl.multiple_of(HALO + z * count + x * rows_own, 16), rows_own)

    def tok_block(z, x):
        return tok.at[tok_rows(z, x)]

    pairs = (
        (tokens_hbm, tok_block(parity, t)),
        (wq_hbm, wq_ref),
        (wk_hbm, kv_ref.at[0]),
        (wv_hbm, kv_ref.at[1]),
        (wb_hbm, wb_ref),
        (wc_hbm, wc_ref),
        (wx_hbm, wx_ref),
        (gate_hbm, gate_own),
        (taps_hbm, taps_own),
        (gain_hbm, gain),
        (oconv_hbm, wout.at[pl.ds(0, 2 * ch)]),
        (oattn_hbm, wout.at[pl.ds(2 * ch, 2 * ch)]),
    )
    loads = [
        pltpu.make_async_copy(src, dst, local_sem.at[k]) for k, (src, dst) in enumerate(pairs)
    ]
    for copy in loads:
        copy.start()

    @pl.when(jnp.logical_not(late))
    def _():
        tok[:HALO, :] = jnp.zeros((HALO, width), BF16)
        pack[0, :, :, :] = jnp.zeros(pack.shape[1:], BF16)

    pl.semaphore_wait(barrier, 2 * n_sp + 1)

    used = [0]
    sent = []

    def send(src, dst, arrival, device, when=None):
        index = used[0]
        used[0] += 1
        copy = pltpu.make_async_remote_copy(
            src_ref=src,
            dst_ref=dst,
            send_sem=send_sem.at[index],
            recv_sem=arrival,
            device_id=device,
            device_id_type=MESH,
        )
        sent.append((copy, when))
        if when is None:
            copy.start()
        else:
            pl.when(when)(copy.start)
        return copy

    def arrived(ref, arrival):
        pltpu.make_async_remote_copy(
            src_ref=ref,
            dst_ref=ref,
            send_sem=send_sem.at[0],
            recv_sem=arrival,
            device_id=across,
            device_id_type=MESH,
        ).wait_recv()

    def tok_send(z, x, devices):
        here = tok_block(z, x)
        for device in devices:
            send(here, here, tok_sem.at[z * n_tp + x], device)

    def tok_wait(z, x):
        arrived(tok_block(z, x), tok_sem.at[z * n_tp + x])

    halo_sem = tok_sem.at[2 * n_tp]
    halo = tok.at[pl.ds(0, HALO)]

    MATS = {"q": 0, "kv": 1, "b": 2, "c": 3, "x": 4}
    lanes = {"q": (q_all, 0), "b": (bc_all, 0), "c": (bc_all, 1), "x": (x_all, 0)}
    local = {"q": wq_ref, "b": wb_ref, "c": wc_ref, "x": wx_ref}

    def w_place(m, z, start, size):
        if m == "kv":
            return kv_all.at[z, :, pl.ds(pl.multiple_of(start, half), size)]
        ref, k = lanes[m]
        rows = pl.ds(pl.multiple_of(z * depth + start, half), size)
        return ref.at[rows, pl.ds(k * ch, ch)]

    def w_source(m, to, start, size):
        if m == "kv":
            return kv_ref.at[to, :, pl.ds(pl.multiple_of(start, half), size)]
        cols = pl.ds(pl.multiple_of(to * ch, ch), ch)
        return local[m].at[pl.ds(pl.multiple_of(start, half), size), cols]

    def w_arrival(m, z, part_of):
        return w_sem.at[MATS[m] * 2 * n_sp + 2 * z + part_of]

    def w_send_far(mats):
        z = jnp.where(owner, z_two, z_three)
        for m in mats:
            for to in range(2):
                send(
                    w_source(m, to, g * half, half),
                    w_place(m, s, g * half, half),
                    w_arrival(m, s, g),
                    {"sp": z, "tp": first + to},
                )

    def w_send_near(mats):
        for m in mats:
            for to in range(2):
                send(
                    w_source(m, to, g * half, half),
                    w_place(m, s, g * half, half),
                    w_arrival(m, s, g),
                    {"sp": z_near, "tp": first + to},
                    jnp.logical_not(owner),
                )

    def w_send_here(mats):
        for m in mats:
            send(
                w_source(m, 1 - core, 0, depth),
                w_place(m, s, 0, depth),
                w_arrival(m, s, 0),
                {"tp": sibling},
                owner,
            )

            @pl.when(owner)
            def _(m=m):
                if m == "kv":
                    kv_all[s, :, :] = kv_ref[core]
                else:
                    ref, k = lanes[m]
                    own = local[m][...]
                    ref[block(s, depth), k * ch : (k + 1) * ch] = jnp.where(
                        core == 0, own[:, :ch], own[:, ch:]
                    )

    def w_over(mats, z):
        for m in mats:
            place = w_place(m, z, g * half, half)
            arrived(place, w_arrival(m, z, g))
            send(place, place, w_arrival(m, z, g), across)

    def w_here(mats):
        for m in mats:

            @pl.when(jnp.logical_not(owner))
            def _(m=m):
                arrived(w_place(m, s, 0, depth), w_arrival(m, s, 0))

    def w_across(mats, z):
        for m in mats:
            arrived(w_place(m, z, (1 - g) * half, half), w_arrival(m, z, 1 - g))

    others = (z_two, z_three, z_near)

    loads[0].wait()
    tok_send(parity, t, ({"sp": z_near}, {"tp": far}, {"tp": sibling}))
    tail_rows = pl.ds(pl.multiple_of(HALO + parity * count + (t + 1) * rows_own - HALO, 16), HALO)
    end = t == n_tp - 1
    send(tok.at[tail_rows], halo, halo_sem, {"sp": 2}, jnp.logical_and(s == 1, end))
    for copy in loads[1:4]:
        copy.wait()
    w_send_far(("q", "kv"))
    w_send_near(("q", "kv"))
    w_send_here(("q", "kv"))
    for copy in loads[4:7]:
        copy.wait()
    w_send_far(("b", "c"))
    w_send_near(("b", "c"))
    for copy in loads[7:10]:
        copy.wait()
    send(gate_own, gate_sib, small_sem.at[0], {"tp": sibling})
    send(taps_own, taps_sib, small_sem.at[1], {"tp": sibling})
    w_send_here(("b", "c", "x"))

    tok_wait(1 - parity, t)
    tok_send(1 - parity, t, ({"tp": far}, {"tp": sibling}))
    tok_wait(parity, far)
    tok_send(parity, far, ({"tp": sibling},))

    late_end = jnp.logical_and(late, end)

    @pl.when(late_end)
    def _():
        arrived(halo, halo_sem)

    send(halo, halo, halo_sem, {"sp": n_sp - 1}, jnp.logical_and(s == 2, end))
    send(halo, halo, halo_sem, {"tp": far}, late_end)
    send(halo, halo, halo_sem, {"tp": sibling}, late_end)
    for z in others:
        w_over(("q", "kv"), z)
    tok_wait(1 - parity, far)
    tok_send(1 - parity, far, ({"tp": sibling},))

    late_rest = jnp.logical_and(late, jnp.logical_not(end))

    @pl.when(late_rest)
    def _():
        arrived(halo, halo_sem)

    send(halo, halo, halo_sem, {"tp": sibling}, jnp.logical_and(late, t == 1))
    for x in (sibling, far_sibling):
        for z in (parity, 1 - parity):
            tok_wait(z, x)

    def normalize(rows, size):
        xf = tok[rows, :].astype(F32)
        square = jnp.sum(xf * xf, axis=-1, keepdims=True)
        normed[rows, :] = (xf * gain[...]).astype(BF16)
        scale[rows, :] = jnp.broadcast_to(
            lax.rsqrt(square / width + 1e-05), (size, scale.shape[1])
        )

    def normalize_block(i, unused):
        normalize(pl.ds(pl.multiple_of(HALO + i * rows_own, 16), rows_own), rows_own)
        return unused

    normalize(pl.ds(0, HALO), HALO)
    lax.fori_loop(0, 2 * n_tp, normalize_block, 0)

    w_here(("q", "kv"))
    for z in others:
        w_across(("q", "kv"), z)
    body = normed[HALO:, :]
    scale_body = scale[HALO:, :]
    query = jnp.dot(body, q_all[...], preferred_element_type=F32)
    query = (query * scale_body).astype(BF16) * BF16(HD**-0.5)
    keyed = jnp.zeros((mine, HD), F32)
    for z in range(n_sp):
        keyed = keyed + lax.dot_general(
            body[:, z * depth : (z + 1) * depth],
            kv_all[z],
            (((1,), (1,)), ((), ())),
            preferred_element_type=F32,
        )
    keyed = (keyed * scale_body[:, :HD]).astype(BF16)
    pack[1, core, :, :] = jnp.concatenate([keyed[:count], keyed[count:]], axis=1)
    early = jnp.logical_not(late)
    for to in range(2):
        send(
            pack.at[1, core],
            pack.at[0, core],
            kv_sem.at[core],
            {"sp": z_two, "tp": first + to},
            early,
        )
    send(pack.at[1, core], pack.at[1, core], kv_sem.at[2 + core], {"tp": sibling})
    w_send_far(("x",))
    w_send_near(("x",))

    for z in others:
        w_over(("b", "c"), z)
    w_here(("b", "c"))
    for z in others:
        w_across(("b", "c"), z)
    both = jnp.dot(normed[...], bc_all[...], preferred_element_type=F32)
    gates[...] = (both * jnp.concatenate([scale[...], scale[...]], axis=1)).astype(BF16)

    arrived(pack.at[1, 1 - core], kv_sem.at[3 - core])
    for k in range(2):

        @pl.when(late)
        def _(k=k):
            arrived(pack.at[0, k], kv_sem.at[k])

    for k, (own, other) in enumerate(((gate_own, gate_sib), (taps_own, taps_sib))):
        arrived(other, small_sem.at[k])
    gate_all = jnp.where(owner, gate_own[...], gate_sib[...])
    gate_two = jnp.where(core == 0, gate_all[:2], gate_all[2:])
    gate_here = jnp.where(late, gate_two[:, mine:], gate_two[:, :mine])
    gate_keys = jnp.concatenate([gate_two[:, :mine], gate_here], axis=1)
    taps_all = jnp.where(owner, taps_own[...], taps_sib[...])
    taps_here = jnp.where(core == 0, taps_all[:, :ch], taps_all[:, ch:])

    def unpacked(k):
        return jnp.concatenate(
            [pack[0, k, :, :HD], pack[0, k, :, HD:], pack[1, k, :, :HD], pack[1, k, :, HD:]],
            axis=0,
        )

    keys, values = unpacked(0), unpacked(1)

    def deliver(kind, out_ref, d, out):
        here = jnp.logical_and(parity == d, owner)
        device = {"sp": jnp.where(parity == d, s, z_near), "tp": first + parity}
        for r in range(2):
            for k in range(n_tp):
                start = k * rows_own + r * sub
                out_ref[r, d, k * sub : (k + 1) * sub] = out[start : start + sub]
            send(
                out_ref.at[r, d],
                comb.at[kind, r, core],
                out_sem.at[kind * 4 + r * 2 + core],
                device,
                jnp.logical_not(here),
            )

            @pl.when(here)
            def _(r=r):
                comb[kind, r, core] = out_ref[r, d]

    for d in (1, 0):
        rows = slice(d * count, (d + 1) * count)
        seen = mine + (d + 1) * count
        q_pos = mine + d * count + lax.broadcasted_iota(jnp.int32, (count, seen), 0)
        k_pos = lax.broadcasted_iota(jnp.int32, (count, seen), 1)
        visible = jnp.logical_and(k_pos <= q_pos, jnp.logical_or(late, k_pos >= mine))
        outs = []
        logs = []
        for j in range(2):
            score = lax.dot_general(
                query[rows, j * HD : (j + 1) * HD],
                keys[:seen],
                (((1,), (1,)), ((), ())),
                preferred_element_type=F32,
            )
            gate_row = gate_here[j : j + 1, rows]
            gate_column = jnp.broadcast_to(gate_row, (LANES, count)).T[:, :1]
            score = score + gate_column - gate_keys[j : j + 1, :seen]
            score = jnp.where(visible, score, -1e30)
            row_max = jnp.max(score, axis=-1, keepdims=True)
            weight = jnp.exp(score - row_max)
            row_sum = jnp.sum(weight, axis=-1, keepdims=True)
            out = jnp.dot(weight.astype(BF16), values[:seen], preferred_element_type=F32)
            outs.append((out / row_sum).astype(BF16))
            log = jnp.broadcast_to(row_max + jnp.log(row_sum), (count, LANES)).T
            logs.append(log[:1])
        deliver(0, attn_o, d, jnp.concatenate(outs, axis=1))
        lse_out[d, :2] = jnp.concatenate(logs, axis=0)
        here = jnp.logical_and(parity == d, owner)
        send(
            lse_out.at[d],
            lse_in.at[core],
            out_sem.at[8 + core],
            {"sp": jnp.where(parity == d, s, z_near), "tp": first + parity},
            jnp.logical_not(here),
        )

        @pl.when(here)
        def _(d=d):
            lse_in[core] = lse_out[d]

    for z in others:
        w_over(("x",), z)
    w_here(("x",))
    for z in others:
        w_across(("x",), z)
    conv_in = jnp.dot(normed[...], x_all[...], preferred_element_type=F32)
    conv_in = (conv_in * scale[...]).astype(BF16).astype(F32)
    conv_src = (gates[:, ch:].astype(F32) * conv_in).astype(BF16).astype(F32)
    taps = taps_hbm.shape[0]
    filtered = jnp.zeros((mine, ch), F32)
    for tap in range(taps):
        back = taps - 1 - tap
        moved = pltpu.roll(conv_src, back, axis=0) if back else conv_src
        filtered = filtered + taps_here[tap : tap + 1] * moved[HALO:]
    conv_out = (gates[HALO:, :ch].astype(F32) * filtered).astype(BF16)
    for d in (1, 0):
        deliver(1, conv_o, d, conv_out[d * count : (d + 1) * count])

    for copy in loads[10:]:
        copy.wait()

    chunks = 2
    wide = width // chunks

    def relay(r, c):
        cols = pl.ds(c * wide, wide)
        base = 3 * (chunks * r + c)
        for k in range(2):
            arrived(sib.at[r, k, :, cols], sum_sem.at[base + k])
        pair = part[r, far, :, cols].astype(F32) + sib[r, 1, :, cols].astype(F32)
        fwd[r, :, cols] = pair.astype(BF16)
        send(fwd.at[r, :, cols], xin.at[r, :, cols], sum_sem.at[base + 2], {"tp": far})

    last = None
    for r in range(2):
        for kind in range(2):
            for k in range(2):

                @pl.when(jnp.logical_not(jnp.logical_and(owner, core == k)))
                def _(kind=kind, r=r, k=k):
                    arrived(comb.at[kind, r, k], out_sem.at[kind * 4 + r * 2 + k])

        gathered = jnp.concatenate(
            [comb[1, r, 0], comb[1, r, 1], comb[0, r, 0], comb[0, r, 1]], axis=1
        )
        for c in range(chunks):
            cols = pl.ds(c * wide, wide)
            term = jnp.dot(gathered, wout[:, cols], preferred_element_type=F32).astype(BF16)
            for k in range(n_tp):
                part[r, k, :, cols] = term[k * sub : (k + 1) * sub]
            for k, to in ((1, far_sibling), (0, sibling)):
                send(
                    part.at[r, to, :, cols],
                    sib.at[r, k, :, cols],
                    sum_sem.at[3 * (chunks * r + c) + k],
                    {"tp": sibling},
                )
            if last is not None:
                relay(*last)
            last = (r, c)
    relay(*last)
    for k in range(2):

        @pl.when(jnp.logical_not(jnp.logical_and(owner, core == k)))
        def _(k=k):
            arrived(lse_in.at[k], out_sem.at[8 + k])

        lse_ref[2 * k : 2 * k + 2, :] = lse_in[k, :2]
    for r in range(2):
        for c in range(chunks):
            cols = pl.ds(c * wide, wide)
            arrived(xin.at[r, :, cols], sum_sem.at[3 * (chunks * r + c) + 2])
            whole = part[r, t, :, cols].astype(F32) + sib[r, 0, :, cols].astype(F32)
            whole = whole + xin[r, :, cols].astype(F32)
            mixed_ref[r * sub : (r + 1) * sub, cols] = whole.astype(BF16)
    for copy, when in sent:
        if when is None:
            copy.wait_send()
        else:
            pl.when(when)(copy.wait_send)


COPIES = 192
HALO = 16


def in_one_kernel(
    n_sp,
    n_tp,
    tokens,
    norm_gain,
    conv_b_w,
    conv_c_w,
    conv_x_w,
    query_w,
    key_w,
    value_w,
    conv_taps,
    gate_cache,
    out_conv_w,
    out_attn_w,
):
    rows, width = tokens.shape
    count = rows * n_tp
    mine = 2 * count
    depth, channels = conv_b_w.shape
    ch = channels // 2
    heads = gate_cache.shape[1]
    vmem = pl.BlockSpec(memory_space=pltpu.VMEM)
    hbm = pl.BlockSpec(memory_space=pl.ANY)
    out_rows = out_conv_w.shape[0] + out_attn_w.shape[0]
    dma = pltpu.SemaphoreType.DMA
    gate_rows = gate_cache.T
    mixed, log_rows = pl.pallas_call(
        functools.partial(layer_kernel, n_sp, n_tp),
        out_shape=(
            jax.ShapeDtypeStruct((rows, width), BF16),
            jax.ShapeDtypeStruct((heads, count), F32),
        ),
        in_specs=[hbm] * 12,
        out_specs=(vmem, vmem),
        scratch_shapes=[
            pltpu.VMEM((HALO + mine, width), BF16),
            pltpu.VMEM((HALO + mine, width), BF16),
            pltpu.VMEM((HALO + mine, LANES), F32),
            pltpu.VMEM((1, width), F32),
            pltpu.VMEM(conv_taps.shape, F32),
            pltpu.VMEM(conv_taps.shape, F32),
            pltpu.VMEM(gate_rows.shape, F32),
            pltpu.VMEM(gate_rows.shape, F32),
            pltpu.VMEM(conv_b_w.shape, BF16),
            pltpu.VMEM(conv_c_w.shape, BF16),
            pltpu.VMEM(conv_x_w.shape, BF16),
            pltpu.VMEM(query_w.shape, BF16),
            pltpu.VMEM((2, key_w.shape[1], depth), BF16),
            pltpu.VMEM((width, 2 * ch), BF16),
            pltpu.VMEM((width, ch), BF16),
            pltpu.VMEM((width, ch), BF16),
            pltpu.VMEM((n_sp, key_w.shape[1], depth), BF16),
            pltpu.VMEM((HALO + mine, 2 * ch), BF16),
            pltpu.VMEM((2, 2, count, 2 * HD), BF16),
            pltpu.VMEM((2, 2, count // 2, ch), BF16),
            pltpu.VMEM((2, 2, count // 2, ch), BF16),
            pltpu.VMEM((2, 2, 2, count // 2, ch), BF16),
            pltpu.VMEM((2, 8, count), F32),
            pltpu.VMEM((2, 8, count), F32),
            pltpu.VMEM((out_rows, width), BF16),
            pltpu.VMEM((2, n_tp, rows // 2, width), BF16),
            pltpu.VMEM((2, 2, rows // 2, width), BF16),
            pltpu.VMEM((2, rows // 2, width), BF16),
            pltpu.VMEM((2, rows // 2, width), BF16),
            dma((COPIES,)),
            dma((2 * n_tp + 1,)),
            dma((5 * 2 * n_sp,)),
            dma((2,)),
            dma((4,)),
            dma((10,)),
            dma((12,)),
            dma((12,)),
        ],
        compiler_params=pltpu.CompilerParams(
            collective_id=0, has_side_effects=True, vmem_limit_bytes=60 * 1024 * 1024
        ),
    )(
        tokens,
        norm_gain.reshape(1, width),
        conv_b_w,
        conv_c_w,
        conv_x_w,
        query_w,
        key_w.T,
        value_w.T,
        conv_taps,
        gate_rows,
        out_conv_w,
        out_attn_w,
    )
    return mixed, log_rows.T


def passed_along(value, axis, by):
    count = lax.axis_size(axis)
    pairs = [(i, i + by) for i in range(count) if 0 <= i + by < count]
    return lax.ppermute(value, axis, pairs)


def on_device(
    tokens,
    norm_gain,
    conv_b_w,
    conv_c_w,
    conv_x_w,
    query_w,
    key_w,
    value_w,
    conv_taps,
    gate_cache,
    out_conv_w,
    out_attn_w,
):
    rows = lax.all_gather(tokens, "tp", axis=0, tiled=True)
    count = rows.shape[0]
    xf = rows.astype(jnp.float32)
    scale_rows = lax.rsqrt(jnp.mean(xf * xf, axis=-1, keepdims=True) + 1e-05)
    normed = (xf * norm_gain).astype(jnp.bfloat16)

    def contract_all(pieces):
        width = pieces[0].shape[0]
        return tuple(
            (jnp.dot(normed, piece, preferred_element_type=jnp.float32) for piece in pieces)
        )

    conv_sums = contract_all(
        (
            lax.all_gather(conv_b_w, "sp", axis=0, tiled=True),
            lax.all_gather(conv_c_w, "sp", axis=0, tiled=True),
            lax.all_gather(conv_x_w, "sp", axis=0, tiled=True),
        )
    )
    attn_sums = contract_all(
        (
            lax.all_gather(query_w, "sp", axis=0, tiled=True),
            lax.all_gather(key_w, "sp", axis=0, tiled=True),
            lax.all_gather(value_w, "sp", axis=0, tiled=True),
        )
    )
    sums = conv_sums + attn_sums
    gate_b, gate_c, conv_in, query, key, value = [
        (total * scale_rows).astype(jnp.bfloat16) for total in sums
    ]
    taps = conv_taps.shape[0]
    channels = conv_in.shape[1]
    conv_src = (gate_c.astype(jnp.float32) * conv_in.astype(jnp.float32)).astype(jnp.bfloat16)
    earlier = passed_along(conv_src[count - (taps - 1) :], "sp", 1)
    padded = jnp.concatenate([earlier, conv_src], axis=0)
    filtered = jnp.zeros((count, channels), jnp.float32)
    for tap in range(taps):
        filtered = filtered + conv_taps[tap][None, :] * padded[tap : tap + count].astype(
            jnp.float32
        )
    conv_out = (gate_b.astype(jnp.float32) * filtered).astype(jnp.bfloat16)
    heads_dev = gate_cache.shape[1]
    kv_dev = key.shape[1] // HD
    group = heads_dev // kv_dev
    half = count // 2
    sp_index = lax.axis_index("sp")
    own_start = sp_index * count
    scale = HD ** (-0.5)
    later_query = query[half:]
    later_start = own_start + half

    def prepare(q_rows, begin):
        heads_q = q_rows.reshape(half, kv_dev, group, HD)
        q_gate = lax.dynamic_slice_in_dim(gate_cache, begin, half, 0).T.reshape(
            kv_dev, group, half, 1
        )
        q_pos = begin + jnp.arange(half, dtype=jnp.int32)
        return (heads_q, q_gate, q_pos)

    sides = (prepare(query[:half], own_start), prepare(later_query, later_start))

    def absorb(carry, side, key_rows, value_rows, begin):
        heads_q, q_gate, q_pos = side
        run_max, run_sum, acc = carry
        width = key_rows.shape[0]
        key_heads = key_rows.reshape(width, kv_dev, HD)
        value_heads = value_rows.reshape(width, kv_dev, HD)
        score = (
            jnp.einsum("qgjd,kgd->gjqk", heads_q, key_heads, preferred_element_type=jnp.float32)
            * scale
        )
        key_gate = lax.dynamic_slice_in_dim(gate_cache, begin, width, 0).T.reshape(
            kv_dev, group, 1, width
        )
        score = score + q_gate - key_gate
        mask = (begin + jnp.arange(width, dtype=jnp.int32))[None, :] <= q_pos[:, None]
        score = jnp.where(mask, score, -1e30)
        new_max = jnp.maximum(run_max, jnp.max(score, axis=-1))
        weight = jnp.where(mask, jnp.exp(score - new_max[..., None]), 0.0)
        factor = jnp.exp(run_max - new_max)
        new_sum = run_sum * factor + jnp.sum(weight, axis=-1)
        product = jnp.einsum(
            "gjqk,kgd->gjqd",
            weight.astype(jnp.bfloat16),
            value_heads,
            preferred_element_type=jnp.float32,
        )
        return (new_max, new_sum, acc * factor[..., None] + product)

    def guarded(carry, side, key_rows, value_rows, begin):

        def visit_rows(state):
            return absorb(state, side, key_rows, value_rows, begin)

        def keep(state):
            return state

        return lax.cond(begin <= side[2][half - 1], visit_rows, keep, carry)

    def absorb_both(carry, key_rows, value_rows, begin):
        return (
            guarded(carry[0], sides[0], key_rows, value_rows, begin),
            guarded(carry[1], sides[1], key_rows, value_rows, begin),
        )

    def fresh():
        return (
            jnp.full((kv_dev, group, half), -1e30, jnp.float32),
            jnp.zeros((kv_dev, group, half), jnp.float32),
            jnp.zeros((kv_dev, group, half, HD), jnp.float32),
        )

    key_rows = lax.all_gather(key, "sp", axis=0, tiled=True)
    value_rows = lax.all_gather(value, "sp", axis=0, tiled=True)
    width = key_rows.shape[0]
    step = 512
    key_blocks = key_rows.reshape(width // step, step, key_rows.shape[1])
    value_blocks = value_rows.reshape(width // step, step, value_rows.shape[1])
    firsts = step * jnp.arange(width // step, dtype=jnp.int32)

    def visit(state, inputs):
        return (absorb_both(state, inputs[0], inputs[1], inputs[2]), None)

    result, unused = lax.scan(visit, (fresh(), fresh()), (key_blocks, value_blocks, firsts))

    def finish(state):
        run_max, run_sum, acc = state
        out = (
            (acc / run_sum[..., None])
            .transpose(2, 0, 1, 3)
            .reshape(half, heads_dev * HD)
            .astype(jnp.bfloat16)
        )
        lse = (run_max + jnp.log(run_sum)).transpose(2, 0, 1).reshape(half, heads_dev)
        return (out, lse)

    early_out, early_lse = finish(result[0])
    later_out, later_lse = finish(result[1])
    attn_out = jnp.concatenate([early_out, later_out], axis=0)
    log_total = jnp.concatenate([early_lse, later_lse], axis=0)
    term = jnp.dot(conv_out, out_conv_w, preferred_element_type=jnp.float32)
    mixed = lax.psum_scatter(
        (term + jnp.dot(attn_out, out_attn_w, preferred_element_type=jnp.float32)).astype(
            jnp.bfloat16
        ),
        "tp",
        scatter_dimension=0,
        tiled=True,
    )
    return (mixed, log_total)


def solution(mesh):
    placed = (
        P(("grp", "sp", "tp"), None),
        P(),
        P("sp", "tp"),
        P("sp", "tp"),
        P("sp", "tp"),
        P("sp", "tp"),
        P("sp", "tp"),
        P("sp", "tp"),
        P(None, "tp"),
        P("grp", "tp"),
        P("tp", None),
        P("tp", None),
    )
    sizes = dict(mesh.shape)

    def on_one(*args):
        channels, key_width = args[2].shape[1], args[6].shape[1]
        grid = (sizes["grp"], sizes["sp"], sizes["tp"])
        fits = channels == 2 * LANES and args[5].shape[1] == channels and key_width == HD
        if grid == (2, 4, 4) and fits and args[9].shape[1] * HD == channels:
            return in_one_kernel(sizes["sp"], sizes["tp"], *args)
        return on_device(*args)

    return jax.shard_map(
        on_one,
        mesh=mesh,
        in_specs=placed,
        out_specs=(P(("grp", "sp", "tp"), None), P(("grp", "sp"), "tp")),
        check_vma=False,
    )
```

time: 69.8 us -> 67.9 us (0.973)
  the two profiles are of different devices: /device:TPU:0 before, /device:TPU:16 now
where the time goes in v1:
time: 67.9 us; the launch traced here: 66.7 us
  Pallas kernels  63.7 us (94%)
  local copies, waits for them, and re-layouts  2.27 us (3%)
    pallas_call x1, Pallas kernels, in_one_kernel(): pl.pallas_call(functools.partial(layer_kernel, n_sp, n_tp), out_shape=(ja...  63.7 us
    unnamed x4, local copies, waits for them, and re-layouts  2.27 us

profile of v1, /device:TPU:16, one launch (start us, length us, event | category | flops | bytes accessed | tf_op | source)
XLA Modules:
  0.0 66.7 jit_solution(14356708525303551108)
XLA Ops:
  0.6 63.7 %shard_map.131 = (bf16[64,2048]{1,0:T(8,128)(2,1)}, f32[4,256]{1,0:T(4,128)}) custom-call(bf16[64,2048]{1,0:T(8,128)(2,1)} %tokens_hbm.1, f32[1,2048]{1,0:T(1,128)} %bitcast.8, bf16[512,256]{1,0:T(8,128)(2,1)} %wb_hbm.1, bf16[512,256]{1,0:T(8,128)(2,1)} %wc_hbm.1, bf16[512,256]{1,0:T(8,128)(2,1)} %wx_hbm.1, bf16[512,256]{1,0:T(8,128)(2,1)} %wq_hbm.1, ...), custom_call_target="tpu_custom_call" | custom-call | tf_op jit(solution)/shard_map/pallas_call | solution.py:568
  64.4 0.0 copy-start
  64.4 1.7 %copy.16 = bf16[64,2048]{1,0:T(8,128)(2,1)} copy(bf16[64,2048]{1,0:T(8,128)(2,1)} %get-tuple-element.8) | data formatting | bytes 524288
  66.1 0.0 copy-done
  66.1 0.6 copy.17
Async XLA Ops:
  64.4 1.7 %copy-start = (f32[4,256]{1,0:T(4,128)S(1)}, f32[4,256]{1,0:T(4,128)}, u32[]{:S(2)}) copy-start(f32[4,256]{1,0:T(4,128)} %get-tuple-element.5) | copy-start | bytes 12292
